TPU v7x, 256 devices: a whole 4x4x8 slice. The times are simulated.
256 devices in a mesh: rep: 2 (over z_hi), fs: 16 (over z_lo, x), tp: 8 (over y, core).
Axes of the slice: x: 4, y: 4, z: 8 (z_hi: 2, z_lo: 4; z = z_hi * 4 + z_lo), core: 2. Of those that a mesh axis runs over, the one named last changes fastest.
Arguments:
- tokens: bfloat16 [32, 1024, 2048], P(('rep', 'fs')), may hold values from -6 to 6
- mix_gain: bfloat16 [2048], replicated, may hold values from 0.099609375 to 1.8984375
- value_weight: bfloat16 [2048, 1024], P('fs', 'tp'), may hold values from -0.125 to 0.125
- gate_weight: bfloat16 [2048, 1024], P('fs', 'tp'), may hold values from -0.125 to 0.125
- mix_taps: bfloat16 [31, 1024], P(None, 'tp'), may hold values from -1 to 1
- head_gain: bfloat16 [1024], P('tp'), may hold values from 0.099609375 to 1.8984375
- out_weight: bfloat16 [1024, 2048], P('fs', 'tp'), may hold values from -0.1875 to 0.1875
- ffn_gain: bfloat16 [2048], replicated, may hold values from 0.099609375 to 1.8984375
- ffgate_weight: bfloat16 [2048, 6144], P('fs', 'tp'), may hold values from -0.125 to 0.125
- up_weight: bfloat16 [2048, 6144], P('fs', 'tp'), may hold values from -0.125 to 0.125
- ff_taps: bfloat16 [3, 6144], P(None, 'tp'), may hold values from -3.5 to 3.5
- down_weight: bfloat16 [2048, 6144], P('fs', 'tp'), may hold values from -0.078125 to 0.078125
Outputs:
- layer_out: bfloat16 [32, 1024, 2048], P(('rep', 'fs'), 'tp')
All inputs are finite; a program needn't handle non-finite values.
Results may differ from a plain program's by a relative error of at most 0.01.
Values may be sent and summed in bfloat16 or wider, within the bound.
A program may use at most 64 MiB of HBM per device.

v0:
```python
import jax
import jax.numpy as jnp
from jax import lax
from jax.sharding import PartitionSpec as P

HEAD = 128
norm_floor = 0.01


def in_one_piece(arrays, axis, dim, along):
    both = jnp.concatenate(arrays, axis=along)
    result, at, finished = (lax.all_gather(both, axis, axis=dim, tiled=True), 0, [])
    for a in arrays:
        finished.append(lax.slice_in_dim(result, at, at + a.shape[along], axis=along))
        at += a.shape[along]
    return tuple(finished)


def laid_out(parts, dim):
    lengths = list(parts.shape[1:])
    lengths[dim] *= parts.shape[0]
    return jnp.moveaxis(parts, 0, dim).reshape(lengths)


def sent_to_all(value, axis):
    count = lax.axis_size(axis)
    return lax.all_to_all(
        jnp.broadcast_to(value[None], (count, *value.shape)), axis, 0, 0, tiled=True
    )


def collect(value, axis, dim):
    return laid_out(sent_to_all(value, axis), dim)


def row_norm(floats_in, scales):
    floats = floats_in.astype(jnp.float32)
    scaled = floats * lax.rsqrt(jnp.mean(floats * floats, axis=-1, keepdims=True) + norm_floor)
    return (scaled * scales.astype(jnp.float32)).astype(jnp.bfloat16)


def causal_conv(signal, kernel_taps):
    reach = kernel_taps.shape[0]
    length = signal.shape[0]
    padded = jnp.pad(signal, ((reach - 1, 0), (0, 0)))
    summed = padded[0:length] * kernel_taps[0]
    for offset in range(1, reach):
        summed = summed + padded[offset : offset + length] * kernel_taps[offset]
    return summed


def head_norm(signal, scales):
    length = signal.shape[0]
    grouped = signal.reshape(length, signal.shape[1] // HEAD, HEAD)
    centre = grouped - jnp.mean(grouped, axis=-1, keepdims=True)
    spread = jnp.mean(centre * centre, axis=-1, keepdims=True)
    normal = (centre * lax.rsqrt(spread + norm_floor)).reshape(signal.shape)
    return normal * scales.astype(jnp.float32)


def on_device(
    tokens,
    mix_gain,
    value_weight,
    gate_weight,
    mix_taps,
    head_gain,
    out_weight,
    ffn_gain,
    ffgate_weight,
    up_weight,
    ff_taps,
    down_weight,
):
    sequence = tokens[0]
    value_full, gate_full, out_full = (
        *in_one_piece((value_weight, gate_weight), "fs", 0, 1),
        lax.all_gather(out_weight, "fs", axis=0, tiled=True),
    )
    normed = row_norm(sequence, mix_gain)
    values = jnp.dot(normed, value_full, preferred_element_type=jnp.float32)
    gating = jnp.dot(normed, gate_full, preferred_element_type=jnp.float32)
    glu_out = values * jax.nn.sigmoid(gating)
    mixed_pos = causal_conv(glu_out, mix_taps.astype(jnp.float32))
    head_out = jax.nn.silu(head_norm(mixed_pos, head_gain)).astype(jnp.bfloat16)
    out_cols = out_full.shape[1]
    mixer_sum = jnp.dot(collect(head_out, "tp", 1), out_full, preferred_element_type=jnp.float32)
    own_cols = lax.dynamic_slice_in_dim(sequence, lax.axis_index("tp") * out_cols, out_cols, 1)
    hidden_cols = (own_cols.astype(jnp.float32) + mixer_sum).astype(jnp.bfloat16)
    full_rows = collect(hidden_cols, "tp", 1)
    normed_ffn = row_norm(full_rows, ffn_gain)
    ffgate_full, up_full, down_full = in_one_piece(
        (ffgate_weight, up_weight, down_weight), "fs", 0, 1
    )
    ffgate = jnp.dot(normed_ffn, ffgate_full, preferred_element_type=jnp.float32)
    ff_up = jnp.dot(normed_ffn, up_full, preferred_element_type=jnp.float32)
    product = (jax.nn.silu(causal_conv(ffgate, ff_taps.astype(jnp.float32))) * ff_up).astype(
        jnp.bfloat16
    )
    own_count = sequence.shape[0] // lax.axis_size("tp")
    summed_rows = lax.psum_scatter(
        lax.dot_general(
            product, down_full, (((1,), (1,)), ((), ())), preferred_element_type=jnp.float32
        ).astype(jnp.bfloat16),
        "tp",
        scatter_dimension=0,
        tiled=True,
    ).astype(jnp.float32)
    own_rows = lax.dynamic_slice_in_dim(full_rows, lax.axis_index("tp") * own_count, own_count, 0)
    return (own_rows.astype(jnp.float32) + summed_rows).astype(jnp.bfloat16)[None]


def solution(mesh):
    placed = (
        P(("rep", "fs"), None, None),
        P(),
        P("fs", "tp"),
        P("fs", "tp"),
        P(None, "tp"),
        P("tp"),
        P("fs", "tp"),
        P(),
        P("fs", "tp"),
        P("fs", "tp"),
        P(None, "tp"),
        P("fs", "tp"),
    )
    return jax.shard_map(
        on_device,
        mesh=mesh,
        in_specs=placed,
        out_specs=P(("rep", "fs"), "tp", None),
        check_vma=False,
    )
```

profile of v0, /device:TPU:2, one launch (start us, length us, event | category | flops | bytes accessed | tf_op | source)
XLA Modules:
  0.0 288.3 jit_solution(5631899836314753559)
XLA Ops:
  6.5 1.4 pad_maximum_fusion.1
  8.0 2.0 pad_maximum_fusion
  10.0 0.7 convert_element_type.73
  10.7 0.7 convert_element_type.70
  11.4 0.7 convert_element_type.72
  12.1 3.1 %fusion = f32[1024]{0:T(1024)S(1)} fusion(bf16[1,1024,2048]{2,1,0:T(8,128)(2,1)} %param.12), kind=kLoop, calls=%fused_computation.2 | loop fusion | flops 6290432 | bytes 4198400 | tf_op jit(solution)/shard_map/reduce_sum | solution.py:38
  15.2 77.5 %all-gather.3.cloned.1.call-done = bf16[2048,256]{1,0:T(8,128)(2,1)} async-done(((bf16[128,256]{1,0:T(8,128)(2,1)}), bf16[2048,256]{1,0:T(8,128)(2,1)}) %all-gather.3.cloned.1.call-update) | async-done | bytes 1048592 | tf_op jit(solution)/shard_map/all_gather | solution.py:12
  92.7 3.8 %fusion.19 = f32[1024,128]{1,0:T(8,128)S(1)} fusion(bf16[1,1024,2048]{2,1,0:T(8,128)(2,1)} %param.12, f32[2048]{0:T(1024)S(1)} %convert_element_type.70, f32[1024]{0:T(1024)S(1)} %add_rsqrt_fusion.2, bf16[2048,256]{1,0:T(8,128)(2,1)} %all-gather.3.cloned.1.call-done), kind=kOutput, calls=%fused_computation.24 | convolution fusion | flops 545652736 | bytes 5255168 | tf_op jit(solution)/shard_map/dot_general | solution.py:82
  96.6 1.3 convolution_multiply_fusion
  98.0 2.3 fusion.48
  100.3 0.4 multiply_reduce_fusion.1
  101.2 1.6 broadcast_in_dim.6
  102.8 4.3 %all-to-all-start = ((bf16[8,1024,128]{1,2,0:T(8,128)(2,1)}), bf16[8,1024,128]{1,2,0:T(8,128)(2,1)S(1)}, u32[]{:S(2)}, u32[]{:S(2)}) async-start(bf16[8,1024,128]{1,2,0:T(8,128)(2,1)} %broadcast_in_dim.6), calls=%async_computation | async-start | bytes 4194304 | tf_op jit(solution)/shard_map/all_to_all | solution.py:27
  107.1 46.9 %all_gather.10 = bf16[1024,256]{1,0:T(8,128)(2,1)S(1)} all-gather(bf16[64,256]{1,0:T(8,128)(2,1)S(1)} %copy-done.1), channel_id=1, replica_groups=mesh['rep'=2,'fs'=16,'tp'=8] {'fs'}, dimensions={0}, use_global_device_ids=true | all-gather | bytes 557056 | tf_op jit(solution)/shard_map/all_gather | solution.py:78
  153.9 1.8 fusion.16
  155.8 2.3 broadcast_in_dim.7
  158.1 5.0 %all-to-all-start.1 = ((bf16[8,1024,256]{2,1,0:T(8,128)(2,1)}), bf16[8,1024,256]{2,1,0:T(8,128)(2,1)}, u32[]{:S(2)}, u32[]{:S(2)}) async-start(bf16[8,1024,256]{2,1,0:T(8,128)(2,1)} %broadcast_in_dim.7), calls=%async_computation.1 | async-start | bytes 8388608 | tf_op jit(solution)/shard_map/all_to_all | solution.py:27
  163.4 49.4 %all-to-all-done.1 = bf16[8,1024,256]{2,1,0:T(8,128)(2,1)} async-done(((bf16[8,1024,256]{2,1,0:T(8,128)(2,1)}), bf16[8,1024,256]{2,1,0:T(8,128)(2,1)}, u32[]{:S(2)}, u32[]{:S(2)}) %all-to-all-start.1) | async-done | bytes 4194336 | tf_op jit(solution)/shard_map/all_to_all | solution.py:27
  212.8 4.8 %copy.16 = bf16[8,128,8,256]{3,2,0,1:T(8,128)(2,1)} copy(bf16[8,128,8,256]{3,2,1,0:T(8,128)(2,1)} %bitcast.40) | data formatting | bytes 8388608 | tf_op jit(solution)/shard_map/reshape | solution.py:22
  217.6 3.1 %multiply_reduce_fusion = f32[1024]{0:T(1024)S(1)} fusion(bf16[8,1024,256]{2,1,0:T(8,128)(2,1)} %all-to-all-done.1), kind=kLoop, calls=%fused_computation.6 | loop fusion | flops 6290432 | bytes 4198400 | tf_op jit(solution)/shard_map/reduce_sum | solution.py:38
  220.8 6.4 %fusion.6 = f32[1024,768]{1,0:T(8,128)S(1)} fusion(bf16[2048,2304]{1,0:T(8,128)(2,1)} %all-gather.5.cloned.1.call-done, bf16[1024,2048]{1,0:T(8,128)(2,1)} %bitcast.82, f32[2048]{0:T(1024)S(1)} %convert_element_type.79, f32[1024]{0:T(1024)S(1)} %add_rsqrt_fusion), kind=kOutput, calls=%fused_computation.11 | convolution fusion | flops 3229614080 | bytes 10498048 | tf_op jit(solution)/shard_map/dot_general | solution.py:95
  227.2 13.3 %convolution_convert_fusion = bf16[1024,2048]{1,0:T(8,128)(2,1)} fusion(bf16[2048,2304]{1,0:T(8,128)(2,1)} %all-gather.5.cloned.1.call-done, f32[1024,768]{1,0:T(8,128)S(1)} %fusion.6, f32[768]{0:T(1024)S(1)} %get-tuple-element.6, f32[768]{0:T(1024)S(1)} %get-tuple-element.7, f32[768]{0:T(1024)S(1)} %get-tuple-element.5, bf16[1024,2048]{1,0:T(8,128)(2,1)} %bitcast.83, ...), kind=kOutput, calls=%fused_computation.7 | convolution fusion | flops 6461587456 | bytes 17847296 | tf_op jit(solution)/shard_map/dot_general | solution.py:102
  240.6 39.1 %reduce-scatter.2.cloned.1.call-done = bf16[128,2048]{1,0:T(8,128)(2,1)} async-done(((bf16[1024,2048]{1,0:T(8,128)(2,1)}), bf16[128,2048]{1,0:T(8,128)(2,1)}) %reduce-scatter.2.cloned.1.call-update) | async-done | bytes 524304 | tf_op jit(solution)/shard_map/reduce_scatter | solution.py:101
  279.6 2.1 fusion.22
  (29 shorter events, 1.1 us)
Async XLA Ops:
  6.5 86.2 %all-gather.3.cloned.1.call-start = ((), (), s32[]{:S(2)}) async-start(), calls=%async_computation.3 | async-start | bytes 1114112 | tf_op jit(solution)/shard_map/all_gather | solution.py:12
  8.0 212.8 %all-gather.5.cloned.1.call-start = ((), (), s32[]{:S(2)}) async-start(), calls=%async_computation.4 | async-start | bytes 10027008 | tf_op jit(solution)/shard_map/all_gather | solution.py:12
  92.7 3.8 %copy-start = (bf16[1,1024,2048]{2,1,0:T(8,128)(2,1)S(1)}, bf16[1,1024,2048]{2,1,0:T(8,128)(2,1)}, u32[]{:S(2)}) copy-start(bf16[1,1024,2048]{2,1,0:T(8,128)(2,1)} %param.12) | copy-start | bytes 12582916
  92.7 3.9 %copy-start.4 = (bf16[2048,256]{1,0:T(8,128)(2,1)S(1)}, bf16[2048,256]{1,0:T(8,128)(2,1)}, u32[]{:S(2)}) copy-start(bf16[2048,256]{1,0:T(8,128)(2,1)} %all-gather.3.cloned.1.call-done) | copy-start | bytes 3145732
  100.3 6.8 %copy-start.1 = (bf16[64,256]{1,0:T(8,128)(2,1)S(1)}, bf16[64,256]{1,0:T(8,128)(2,1)}, u32[]{:S(2)}) copy-start(bf16[64,256]{1,0:T(8,128)(2,1)} %param.18) | copy-start | bytes 98308
  102.8 51.2 %all-to-all-start = ((bf16[8,1024,128]{1,2,0:T(8,128)(2,1)}), bf16[8,1024,128]{1,2,0:T(8,128)(2,1)S(1)}, u32[]{:S(2)}, u32[]{:S(2)}) async-start(bf16[8,1024,128]{1,2,0:T(8,128)(2,1)} %broadcast_in_dim.6), calls=%async_computation | async-start | bytes 4194304 | tf_op jit(solution)/shard_map/all_to_all | solution.py:27
  158.1 5.2 %copy-start.3 = (bf16[2048]{0:T(1024)(128)(2,1)S(1)}, bf16[2048]{0:T(1024)(128)(2,1)}, u32[]{:S(2)}) copy-start(bf16[2048]{0:T(1024)(128)(2,1)} %param.19) | copy-start | bytes 12292
  158.1 5.2 %copy-start.2 = (bf16[3,768]{1,0:T(4,128)(2,1)S(1)}, bf16[3,768]{1,0:T(4,128)(2,1)}, u32[]{:S(2)}) copy-start(bf16[3,768]{1,0:T(4,128)(2,1)} %param.22) | copy-start | bytes 13828
  158.1 54.7 %all-to-all-start.1 = ((bf16[8,1024,256]{2,1,0:T(8,128)(2,1)}), bf16[8,1024,256]{2,1,0:T(8,128)(2,1)}, u32[]{:S(2)}, u32[]{:S(2)}) async-start(bf16[8,1024,256]{2,1,0:T(8,128)(2,1)} %broadcast_in_dim.7), calls=%async_computation.1 | async-start | bytes 8388608 | tf_op jit(solution)/shard_map/all_to_all | solution.py:27
  163.1 116.6 %reduce-scatter.2.cloned.1.call-start = ((), (), s32[]{:S(2)}) async-start(), calls=%async_computation.5 | async-start | bytes 4718592 | tf_op jit(solution)/shard_map/reduce_scatter | solution.py:101
Sparse Core Ops, SparseCore 0:
  9.1 83.5 all-gather.2
  94.5 114.2 all-gather.4
  240.7 38.8 reduce-scatter.1
where the time goes:
time: 289 us; the launch traced here: 288 us
  waiting for transfers between devices  166 us (57%)
  blocking collectives  46.9 us (16%)
  matrix products  26.7 us (9%)
  other arithmetic  16.8 us (6%)
  between operations  13.3 us (5%)
  starting transfers between devices  9.5 us (3%)
  local copies, waits for them, and re-layouts  9.09 us (3%)
    all_gather x2, waiting for transfers between devices, in_one_piece(): lax.all_gather(both, axis, axis=dim, tiled=True)  77.6 us
    all_to_all x2, waiting for transfers between devices, sent_to_all(): lax.all_to_all(jnp.broadcast_to(value[None], (count, *value.shape)), axis...  49.4 us
    all_gather x1, blocking collectives, on_device(): lax.all_gather(out_weight, 'fs', axis=0, tiled=True)  46.9 us
    reduce_scatter x1, waiting for transfers between devices, on_device(): lax.psum_scatter(lax.dot_general(product, down_full, (((1,), (1,)), ((),...  39.1 us
    dot_general x1, matrix products, on_device(): lax.dot_general(product, down_full, (((1,), (1,)), ((), ())), preferred_e...  13.3 us
    all_to_all x2, starting transfers between devices, sent_to_all(): lax.all_to_all(jnp.broadcast_to(value[None], (count, *value.shape)), axis...  9.24 us
    dot_general x1, matrix products, on_device(): jnp.dot(normed_ffn, ffgate_full, preferred_element_type=jnp.float32)  6.42 us
    reduce_sum x2, other arithmetic, row_norm(): jnp.mean(floats * floats, axis=-1, keepdims=True) + norm_floor  6.14 us
  transfers between devices with their start and end apart: 5, of which 3 were waited for; matrix products, arithmetic and copies ran while one was open for 10% of the time, Pallas kernels for 0%

commit v1 on v0

--- a/solution.py
+++ b/solution.py
@@ -5,6 +5,11 @@
 
 HEAD = 128
 norm_floor = 0.01
+
+
+def gather_over(x, axis, dim):
+    repeated = jnp.stack([x] * lax.axis_size(axis))
+    return jnp.concatenate(lax.all_to_all(repeated, axis, 0, 0), axis=dim)
 
 
 def in_one_piece(arrays, axis, dim, along):
@@ -75,7 +80,7 @@
     sequence = tokens[0]
     value_full, gate_full, out_full = (
         *in_one_piece((value_weight, gate_weight), "fs", 0, 1),
-        lax.all_gather(out_weight, "fs", axis=0, tiled=True),
+        gather_over(out_weight, "fs", 0),
     )
     normed = row_norm(sequence, mix_gain)
     values = jnp.dot(normed, value_full, preferred_element_type=jnp.float32)

time: 289 us -> 273 us (0.945)
  blocking collectives: 46.9 us -> 0 us
  waiting for transfers between devices: 166 us -> 187 us
  starting transfers between devices: 9.5 us -> 18.1 us
    all_gather x1 -> x0, blocking collectives: 46.9 us -> none  [on_device(): lax.all_gather(out_weight, 'fs', axis=0, tiled=True)]
    all_to_all x2, waiting for transfers between devices: 49.4 us -> 76.5 us  [sent_to_all(): lax.all_to_all(jnp.broadcast_to(value[None], (count, *value.shape)), axis...]
    all_to_all x0 -> x1, starting transfers between devices: none -> 8.91 us  [gather_over(): return jnp.concatenate(lax.all_to_all(repeated, axis, 0, 0), axis=dim)]
    all_gather x2, waiting for transfers between devices: 77.6 us -> 69.8 us  [in_one_piece(): lax.all_gather(both, axis, axis=dim, tiled=True)]
  transfers between devices with their start and end apart: 5 -> 6, of which waited for: 3 -> 5; matrix products, arithmetic and copies ran while one was open for 10% -> 11% of each run, Pallas kernels for 0% -> 0%
where the time goes in v1:
time: 273 us; the launch traced here: 272 us
  waiting for transfers between devices  187 us (68%)
  matrix products  26.6 us (10%)
  starting transfers between devices  18.1 us (7%)
  other arithmetic  16.8 us (6%)
  between operations  13.3 us (5%)
  local copies, waits for them, and re-layouts  10.7 us (4%)
    all_to_all x2, waiting for transfers between devices, sent_to_all(): lax.all_to_all(jnp.broadcast_to(value[None], (count, *value.shape)), axis...  76.5 us
    all_gather x2, waiting for transfers between devices, in_one_piece(): lax.all_gather(both, axis, axis=dim, tiled=True)  69.8 us
    reduce_scatter x1, waiting for transfers between devices, on_device(): lax.psum_scatter(lax.dot_general(product, down_full, (((1,), (1,)), ((),...  40.2 us
    dot_general x1, matrix products, on_device(): lax.dot_general(product, down_full, (((1,), (1,)), ((), ())), preferred_e...  13.3 us
    all_to_all x2, starting transfers between devices, sent_to_all(): lax.all_to_all(jnp.broadcast_to(value[None], (count, *value.shape)), axis...  8.95 us
    all_to_all x1, starting transfers between devices, gather_over(): return jnp.concatenate(lax.all_to_all(repeated, axis, 0, 0), axis=dim)  8.91 us
    dot_general x1, matrix products, on_device(): jnp.dot(normed_ffn, ffgate_full, preferred_element_type=jnp.float32)  6.39 us
    reduce_sum x2, other arithmetic, row_norm(): jnp.mean(floats * floats, axis=-1, keepdims=True) + norm_floor  6.2 us
  transfers between devices with their start and end apart: 6, of which 5 were waited for; matrix products, arithmetic and copies ran while one was open for 11% of the time, Pallas kernels for 0%

profile of v1, /device:TPU:2, one launch (start us, length us, event | category | flops | bytes accessed | tf_op | source)
XLA Modules:
  0.0 272.1 jit_solution(8109473629037071336)
XLA Ops:
  6.5 1.4 pad_maximum_fusion.1
  8.0 2.0 pad_maximum_fusion
  10.0 1.6 stack.2
  11.6 8.9 %all-to-all-start.1 = ((bf16[16,64,256]{2,1,0:T(8,128)(2,1)}), bf16[16,64,256]{2,1,0:T(8,128)(2,1)S(1)}, u32[]{:S(2)}, u32[]{:S(2)}) async-start(bf16[16,64,256]{2,1,0:T(8,128)(2,1)} %stack.2), calls=%async_computation.1 | async-start | bytes 1048576 | tf_op jit(solution)/shard_map/all_to_all | solution.py:12
  21.9 0.7 convert_element_type.72
  22.6 3.1 %fusion = f32[1024]{0:T(1024)S(1)} fusion(bf16[1,1024,2048]{2,1,0:T(8,128)(2,1)} %param.12), kind=kLoop, calls=%fused_computation.2 | loop fusion | flops 6290432 | bytes 4198400 | tf_op jit(solution)/shard_map/reduce_sum | solution.py:43
  25.7 67.0 %all-gather.3.cloned.1.call-done = bf16[2048,256]{1,0:T(8,128)(2,1)} async-done(((bf16[128,256]{1,0:T(8,128)(2,1)}), bf16[2048,256]{1,0:T(8,128)(2,1)}) %all-gather.3.cloned.1.call-update) | async-done | bytes 1048592 | tf_op jit(solution)/shard_map/all_gather | solution.py:17
  92.7 3.8 %fusion.19 = f32[1024,128]{1,0:T(8,128)S(1)} fusion(bf16[1,1024,2048]{2,1,0:T(8,128)(2,1)} %param.12, f32[2048]{0:T(1024)S(1)} %convert_element_type.70, f32[1024]{0:T(1024)S(1)} %add_rsqrt_fusion.2, bf16[2048,256]{1,0:T(8,128)(2,1)} %all-gather.3.cloned.1.call-done), kind=kOutput, calls=%fused_computation.24 | convolution fusion | flops 545652736 | bytes 5255168 | tf_op jit(solution)/shard_map/dot_general | solution.py:87
  96.6 1.3 convolution_multiply_fusion
  97.9 2.3 fusion.48
  101.2 1.6 broadcast_in_dim.6
  102.7 4.3 %all-to-all-start = ((bf16[8,1024,128]{1,2,0:T(8,128)(2,1)}), bf16[8,1024,128]{1,2,0:T(8,128)(2,1)S(1)}, u32[]{:S(2)}, u32[]{:S(2)}) async-start(bf16[8,1024,128]{1,2,0:T(8,128)(2,1)} %broadcast_in_dim.6), calls=%async_computation | async-start | bytes 4194304 | tf_op jit(solution)/shard_map/all_to_all | solution.py:32
  107.0 27.2 %all-to-all-done = bf16[8,1024,128]{1,2,0:T(8,128)(2,1)S(1)} async-done(((bf16[8,1024,128]{1,2,0:T(8,128)(2,1)}), bf16[8,1024,128]{1,2,0:T(8,128)(2,1)S(1)}, u32[]{:S(2)}, u32[]{:S(2)}) %all-to-all-start) | async-done | bytes 2097184 | tf_op jit(solution)/shard_map/all_to_all | solution.py:32
  134.2 1.8 fusion.16
  136.0 2.3 broadcast_in_dim.7
  138.3 4.7 %all-to-all-start.2 = ((bf16[8,1024,256]{2,1,0:T(8,128)(2,1)}), bf16[8,1024,256]{2,1,0:T(8,128)(2,1)}, u32[]{:S(2)}, u32[]{:S(2)}) async-start(bf16[8,1024,256]{2,1,0:T(8,128)(2,1)} %broadcast_in_dim.7), calls=%async_computation.2 | async-start | bytes 8388608 | tf_op jit(solution)/shard_map/all_to_all | solution.py:32
  143.3 49.3 %all-to-all-done.2 = bf16[8,1024,256]{2,1,0:T(8,128)(2,1)} async-done(((bf16[8,1024,256]{2,1,0:T(8,128)(2,1)}), bf16[8,1024,256]{2,1,0:T(8,128)(2,1)}, u32[]{:S(2)}, u32[]{:S(2)}) %all-to-all-start.2) | async-done | bytes 4194336 | tf_op jit(solution)/shard_map/all_to_all | solution.py:32
  192.7 4.9 %copy.16 = bf16[8,128,8,256]{3,2,0,1:T(8,128)(2,1)} copy(bf16[8,128,8,256]{3,2,1,0:T(8,128)(2,1)} %bitcast.41) | data formatting | bytes 8388608 | tf_op jit(solution)/shard_map/reshape | solution.py:27
  197.5 3.1 %multiply_reduce_fusion = f32[1024]{0:T(1024)S(1)} fusion(bf16[8,1024,256]{2,1,0:T(8,128)(2,1)} %all-to-all-done.2), kind=kLoop, calls=%fused_computation.6 | loop fusion | flops 6290432 | bytes 4198400 | tf_op jit(solution)/shard_map/reduce_sum | solution.py:43
  200.7 2.8 %all-gather.5.cloned.1.call-done = bf16[2048,2304]{1,0:T(8,128)(2,1)} async-done(((bf16[128,2304]{1,0:T(8,128)(2,1)}), bf16[2048,2304]{1,0:T(8,128)(2,1)}) %all-gather.5.cloned.1.call-update) | async-done | bytes 9437200 | tf_op jit(solution)/shard_map/all_gather | solution.py:17
  203.5 6.4 %fusion.6 = f32[1024,768]{1,0:T(8,128)S(1)} fusion(bf16[2048,2304]{1,0:T(8,128)(2,1)} %all-gather.5.cloned.1.call-done, bf16[1024,2048]{1,0:T(8,128)(2,1)} %bitcast.83, f32[2048]{0:T(1024)S(1)} %convert_element_type.79, f32[1024]{0:T(1024)S(1)} %add_rsqrt_fusion), kind=kOutput, calls=%fused_computation.11 | convolution fusion | flops 3229614080 | bytes 10498048 | tf_op jit(solution)/shard_map/dot_general | solution.py:100
  209.9 13.3 %convolution_convert_fusion = bf16[1024,2048]{1,0:T(8,128)(2,1)} fusion(bf16[2048,2304]{1,0:T(8,128)(2,1)} %all-gather.5.cloned.1.call-done, f32[1024,768]{1,0:T(8,128)S(1)} %fusion.6, f32[768]{0:T(1024)S(1)} %get-tuple-element.6, f32[768]{0:T(1024)S(1)} %get-tuple-element.7, f32[768]{0:T(1024)S(1)} %get-tuple-element.5, bf16[1024,2048]{1,0:T(8,128)(2,1)} %bitcast.84, ...), kind=kOutput, calls=%fused_computation.7 | convolution fusion | flops 6461587456 | bytes 17847296 | tf_op jit(solution)/shard_map/dot_general | solution.py:107
  223.2 40.2 %reduce-scatter.2.cloned.1.call-done = bf16[128,2048]{1,0:T(8,128)(2,1)} async-done(((bf16[1024,2048]{1,0:T(8,128)(2,1)}), bf16[128,2048]{1,0:T(8,128)(2,1)}) %reduce-scatter.2.cloned.1.call-update) | async-done | bytes 524304 | tf_op jit(solution)/shard_map/reduce_scatter | solution.py:106
  263.4 2.1 fusion.22
  (29 shorter events, 2.7 us)
Async XLA Ops:
  6.5 86.2 %all-gather.3.cloned.1.call-start = ((), (), s32[]{:S(2)}) async-start(), calls=%async_computation.4 | async-start | bytes 1114112 | tf_op jit(solution)/shard_map/all_gather | solution.py:17
  8.0 195.5 %all-gather.5.cloned.1.call-start = ((), (), s32[]{:S(2)}) async-start(), calls=%async_computation.5 | async-start | bytes 10027008 | tf_op jit(solution)/shard_map/all_gather | solution.py:17
  11.6 89.5 %all-to-all-start.1 = ((bf16[16,64,256]{2,1,0:T(8,128)(2,1)}), bf16[16,64,256]{2,1,0:T(8,128)(2,1)S(1)}, u32[]{:S(2)}, u32[]{:S(2)}) async-start(bf16[16,64,256]{2,1,0:T(8,128)(2,1)} %stack.2), calls=%async_computation.1 | async-start | bytes 1048576 | tf_op jit(solution)/shard_map/all_to_all | solution.py:12
  92.7 3.8 %copy-start = (bf16[1,1024,2048]{2,1,0:T(8,128)(2,1)S(1)}, bf16[1,1024,2048]{2,1,0:T(8,128)(2,1)}, u32[]{:S(2)}) copy-start(bf16[1,1024,2048]{2,1,0:T(8,128)(2,1)} %param.12) | copy-start | bytes 12582916
  92.7 3.9 %copy-start.3 = (bf16[2048,256]{1,0:T(8,128)(2,1)S(1)}, bf16[2048,256]{1,0:T(8,128)(2,1)}, u32[]{:S(2)}) copy-start(bf16[2048,256]{1,0:T(8,128)(2,1)} %all-gather.3.cloned.1.call-done) | copy-start | bytes 3145732
  102.7 31.4 %all-to-all-start = ((bf16[8,1024,128]{1,2,0:T(8,128)(2,1)}), bf16[8,1024,128]{1,2,0:T(8,128)(2,1)S(1)}, u32[]{:S(2)}, u32[]{:S(2)}) async-start(bf16[8,1024,128]{1,2,0:T(8,128)(2,1)} %broadcast_in_dim.6), calls=%async_computation | async-start | bytes 4194304 | tf_op jit(solution)/shard_map/all_to_all | solution.py:32
  138.3 4.9 %copy-start.2 = (bf16[2048]{0:T(1024)(128)(2,1)S(1)}, bf16[2048]{0:T(1024)(128)(2,1)}, u32[]{:S(2)}) copy-start(bf16[2048]{0:T(1024)(128)(2,1)} %param.19) | copy-start | bytes 12292
  138.3 4.9 %copy-start.1 = (bf16[3,768]{1,0:T(4,128)(2,1)S(1)}, bf16[3,768]{1,0:T(4,128)(2,1)}, u32[]{:S(2)}) copy-start(bf16[3,768]{1,0:T(4,128)(2,1)} %param.22) | copy-start | bytes 13828
  138.3 54.3 %all-to-all-start.2 = ((bf16[8,1024,256]{2,1,0:T(8,128)(2,1)}), bf16[8,1024,256]{2,1,0:T(8,128)(2,1)}, u32[]{:S(2)}, u32[]{:S(2)}) async-start(bf16[8,1024,256]{2,1,0:T(8,128)(2,1)} %broadcast_in_dim.7), calls=%async_computation.2 | async-start | bytes 8388608 | tf_op jit(solution)/shard_map/all_to_all | solution.py:32
  143.0 120.4 %reduce-scatter.2.cloned.1.call-start = ((), (), s32[]{:S(2)}) async-start(), calls=%async_computation.6 | async-start | bytes 4718592 | tf_op jit(solution)/shard_map/reduce_scatter | solution.py:106
Sparse Core Ops, SparseCore 0:
  9.1 83.5 all-gather.2
  94.5 108.9 all-gather.4
  223.4 40.0 reduce-scatter.1
